TPU v7x, 32 devices: a whole 2x2x4 slice. The times are simulated.
32 devices in a mesh: sp: 8 (over z, x), tp: 4 (over y, core).
Axes of the slice: x: 2, y: 2, z: 4, core: 2. Of those that a mesh axis runs over, the one named last changes fastest.
Arguments:
- residual: bfloat16 [2048, 2048], P(('sp', 'tp')), may hold values from -6 to 6
- queries: bfloat16 [2048, 1024], P('sp', 'tp'), may hold values from -8 to 8
- key_pairs: bfloat16 [2048, 512], P('sp', 'tp'), may hold values from -8 to 8
- values: bfloat16 [2048, 512], P('sp', 'tp'), may hold values from -6 to 6
- lambdas: float32 [8], P('tp'), may hold values from 0.3 to 0.8
- head_gain: float32 [128], replicated, may hold values from 0.1 to 1.9
- out_weight: bfloat16 [1024, 2048], replicated, may hold values from -0.1875 to 0.1875
- mixer_gain: float32 [2048], replicated, may hold values from 0.1 to 1.9
- before_gain: float32 [2048], replicated, may hold values from 0.1 to 1.9
- after_gain: float32 [2048], replicated, may hold values from 0.1 to 1.9
- gate_weight: bfloat16 [2048, 5632], P('sp', 'tp'), may hold values from -0.125 to 0.125
- up_weight: bfloat16 [2048, 5632], P('sp', 'tp'), may hold values from -0.125 to 0.125
- down_weight: bfloat16 [5632, 2048], P('tp', 'sp'), may hold values from -0.078125 to 0.078125
Outputs:
- updated: bfloat16 [2048, 2048], P(('sp', 'tp'))
All inputs are finite; a program needn't handle non-finite values.
Results may differ from a plain program's by a relative error of at most 0.014.
Values may be sent and summed in bfloat16 or wider, within the bound.
A program may use at most 128 MiB of HBM per device.

v0:
```python
import math
import jax
import jax.numpy as jnp
from jax import lax
from jax.sharding import PartitionSpec as P

HEAD_DIM = 64


def row_norm(values_in, gain, epsilon):
    mean_square = jnp.mean(values_in * values_in, axis=-1, keepdims=True)
    return values_in * lax.rsqrt(mean_square + epsilon) * gain


def on_device(
    residual,
    queries,
    key_pairs,
    values,
    lambdas,
    head_gain,
    out_weight,
    mixer_gain,
    before_gain,
    after_gain,
    gate_weight,
    up_weight,
    down_weight,
):
    tokens_here = queries.shape[0]
    quarter = residual.shape[0]
    width = 2 * HEAD_DIM
    local_heads = queries.shape[1] // width
    scale = 1.0 / math.sqrt(HEAD_DIM)
    height = local_heads * tokens_here
    query_rows = jnp.transpose(
        queries.reshape(tokens_here, local_heads, 2, HEAD_DIM), (2, 1, 0, 3)
    ).reshape(2, height, HEAD_DIM)
    empty = (
        jnp.full((height,), -1e30, jnp.float32),
        jnp.zeros((height,), jnp.float32),
        jnp.zeros((height, width), jnp.float32),
    )
    state = (empty, empty)
    key_piece = lax.all_gather(key_pairs, "sp", axis=0, tiled=True)
    value_piece = lax.all_gather(values, "sp", axis=0, tiled=True)
    length = key_piece.shape[0]
    span = length
    for split_count in range(1, length + 1):
        if length % split_count == 0 and length // split_count <= 2048:
            span = length // split_count
            break
    key_blocks = key_piece.reshape(length // span, span, 2, HEAD_DIM)
    value_blocks = value_piece.reshape(length // span, span, width)

    def advance(carry, blocks_in):
        key_block, value_block = blocks_in
        renewed = []
        for which in range(2):
            running_top, running_total, running_numer = carry[which]
            score = (
                jnp.dot(
                    query_rows[which], key_block[:, which].T, preferred_element_type=jnp.float32
                )
                * scale
            )
            new_top = jnp.maximum(running_top, jnp.max(score, axis=1))
            shrink = jnp.exp(running_top - new_top)
            expo = jnp.exp(score - new_top[:, None])
            new_total = running_total * shrink + jnp.sum(expo, axis=1)
            new_numer = running_numer * shrink[:, None] + jnp.dot(
                expo.astype(jnp.bfloat16), value_block, preferred_element_type=jnp.float32
            )
            renewed.append((new_top, new_total, new_numer))
        return (tuple(renewed), None)

    state, _ = lax.scan(advance, state, (key_blocks, value_blocks))
    first_map, second_map = state
    lambda_rows = jnp.repeat(lambdas, tokens_here)[:, None]
    attended = first_map[2] / first_map[1][:, None] - lambda_rows * (
        second_map[2] / second_map[1][:, None]
    )
    normed = row_norm(attended, head_gain, 1e-05).astype(jnp.bfloat16)
    head_out = jnp.transpose(normed.reshape(local_heads, tokens_here, width), (1, 0, 2)).reshape(
        tokens_here, local_heads * width
    )
    grouped = head_out.reshape(lax.axis_size("tp"), quarter, local_heads * width)
    mixed = jnp.dot(
        lax.all_to_all(grouped, "tp", split_axis=0, concat_axis=2, tiled=True)[0],
        out_weight,
        preferred_element_type=jnp.float32,
    ).astype(jnp.bfloat16)[None][0]
    stream = residual.astype(jnp.float32) + row_norm(mixed.astype(jnp.float32), mixer_gain, 1e-06)
    normed_in = row_norm(stream, before_gain, 1e-06).astype(jnp.bfloat16)
    gathered = lax.all_gather(normed_in, "tp", axis=0, tiled=True)
    empty_hidden = jnp.zeros((gathered.shape[0], gate_weight.shape[1]), jnp.float32)
    pieces = (
        lax.all_gather(gate_weight, "sp", axis=0, tiled=True),
        lax.all_gather(up_weight, "sp", axis=0, tiled=True),
    )
    columns = lax.slice_in_dim(gathered, 0, pieces[0].shape[0], axis=1)
    gate_part = jnp.dot(columns, pieces[0], preferred_element_type=jnp.float32)
    up_part = jnp.dot(columns, pieces[1], preferred_element_type=jnp.float32)
    gate = empty_hidden + gate_part
    up = empty_hidden + up_part
    down_whole = lax.all_gather(down_weight, "sp", axis=1, tiled=True)
    hidden = (jax.nn.silu(gate) * up).astype(jnp.bfloat16)
    picked = lax.slice_in_dim(hidden, 0, lax.axis_size("tp") * quarter, axis=0)
    channel = lax.psum_scatter(
        jnp.dot(picked, down_whole, preferred_element_type=jnp.float32).astype(jnp.bfloat16),
        "tp",
        scatter_dimension=0,
        tiled=True,
    )
    updated = stream + 0.5 * row_norm(channel.astype(jnp.float32), after_gain, 1e-06)
    return updated.astype(jnp.bfloat16)


def solution(mesh):
    return jax.shard_map(
        on_device,
        mesh=mesh,
        in_specs=(
            P(("sp", "tp"), None),
            P("sp", "tp"),
            P("sp", "tp"),
            P("sp", "tp"),
            P("tp"),
            P(),
            P(),
            P(),
            P(),
            P(),
            P("sp", "tp"),
            P("sp", "tp"),
            P("tp", "sp"),
        ),
        out_specs=P(("sp", "tp"), None),
        check_vma=False,
    )
```

profile of v0, /device:TPU:0, one launch (start us, length us, event | category | flops | bytes accessed | tf_op | source)
XLA Modules:
  0.0 430.2 jit_solution(3633528644462433819)
XLA Ops:
  6.5 0.9 copy.16
  7.5 33.0 %all_gather.18 = bf16[2048,128]{0,1:T(8,128)(2,1)S(1)} all-gather(bf16[256,128]{0,1:T(8,128)(2,1)S(1)} %copy.16), channel_id=1, replica_groups=mesh['sp'=8,'tp'=4] {'sp'}, dimensions={0}, use_global_device_ids=true | all-gather | bytes 589824 | tf_op jit(solution)/shard_map/all_gather | solution.py:45
  40.5 1.0 copy.14
  41.7 0.8 multiply_reduce_fusion.1
  42.5 0.8 fusion
  43.3 31.3 %all_gather.19 = bf16[2048,128]{1,0:T(8,128)(2,1)S(1)} all-gather(bf16[256,128]{1,0:T(8,128)(2,1)S(1)} %copy-done.3), channel_id=1, replica_groups=mesh['sp'=8,'tp'=4] {'sp'}, dimensions={0}, use_global_device_ids=true | all-gather | bytes 589824 | tf_op jit(solution)/shard_map/all_gather | solution.py:46
  74.7 0.8 multiply_reduce_fusion
  75.5 0.8 fusion.2
  76.5 0.9 fusion.29
  77.4 1.5 multiply_reduce_fusion.4
  79.3 7.2 %all_to_all.15 = bf16[4,64,256]{2,1,0:T(8,128)(2,1)S(1)} all-to-all(bf16[4,64,256]{2,1,0:T(8,128)(2,1)S(1)} %reshape_reshape.3), channel_id=1, replica_groups=mesh['sp'=8,'tp'=4] {'tp'}, dimensions={0} | all-to-all | bytes 262144 | tf_op jit(solution)/shard_map/all_to_all | solution.py:89
  86.6 3.1 multiply_reduce_fusion.3
  90.1 0.9 multiply_convert_fusion
  91.0 0.7 all-gather.7.cloned.1.call-update
  91.8 0.7 all-gather.11.cloned.1.call-update
  93.1 15.0 %all-gather.5.cloned.1.call-done = bf16[256,2048]{1,0:T(8,128)(2,1)} async-done(((bf16[64,2048]{1,0:T(8,128)(2,1)}), bf16[256,2048]{1,0:T(8,128)(2,1)}) %all-gather.5.cloned.1.call-update) | async-done | bytes 1048592 | tf_op jit(solution)/shard_map/all_gather | solution.py:95
  108.1 94.5 %all-gather.7.cloned.1.call-done = bf16[2048,1408]{1,0:T(8,128)(2,1)} async-done(((bf16[256,1408]{1,0:T(8,128)(2,1)}), bf16[2048,1408]{1,0:T(8,128)(2,1)}) %all-gather.7.cloned.1.call-update) | async-done | bytes 5767184 | tf_op jit(solution)/shard_map/all_gather | solution.py:98
  202.6 4.8 %fusion.45 = f32[256,1408]{1,0:T(8,128)S(1)} fusion(bf16[256,2048]{1,0:T(8,128)(2,1)} %all-gather.5.cloned.1.call-done, bf16[2048,1408]{1,0:T(8,128)(2,1)} %all-gather.7.cloned.1.call-done), kind=kOutput, calls=%fused_computation.58 | convolution fusion | flops 1476395008 | bytes 8257536 | tf_op jit(solution)/shard_map/dot_general | solution.py:102
  207.4 88.6 %all-gather.11.cloned.1.call-done = bf16[1408,2048]{1,0:T(8,128)(2,1)} async-done(((bf16[1408,256]{1,0:T(8,128)(2,1)}), bf16[1408,2048]{1,0:T(8,128)(2,1)}) %all-gather.11.cloned.1.call-update) | async-done | bytes 5767184 | tf_op jit(solution)/shard_map/all_gather | solution.py:106
  296.0 92.6 %all-gather.9.cloned.1.call-done = bf16[2048,1408]{1,0:T(8,128)(2,1)} async-done(((bf16[256,1408]{1,0:T(8,128)(2,1)}), bf16[2048,1408]{1,0:T(8,128)(2,1)}) %all-gather.9.cloned.1.call-update) | async-done | bytes 5767184 | tf_op jit(solution)/shard_map/all_gather | solution.py:99
  388.6 8.9 %convolution_convert_fusion = bf16[256,2048]{1,0:T(8,128)(2,1)} fusion(bf16[1408,2048]{1,0:T(8,128)(2,1)} %all-gather.11.cloned.1.call-done, bf16[256,2048]{1,0:T(8,128)(2,1)S(1)} %copy-done.7, bf16[2048,1408]{1,0:T(8,128)(2,1)} %all-gather.9.cloned.1.call-done, f32[256,1408]{1,0:T(8,128)S(1)} %fusion.45), kind=kOutput, calls=%fused_computation.10 | convolution fusion | flops 2955476992 | bytes 15073280 | tf_op jit(solution)/shard_map/dot_general | solution.py:110
  397.5 23.1 %reduce-scatter.2.cloned.1.call-done = bf16[64,2048]{1,0:T(8,128)(2,1)} async-done(((bf16[256,2048]{1,0:T(8,128)(2,1)}), bf16[64,2048]{1,0:T(8,128)(2,1)}) %reduce-scatter.2.cloned.1.call-update) | async-done | bytes 262160 | tf_op jit(solution)/shard_map/reduce_scatter | solution.py:109
  420.6 1.1 fusion.32
  421.7 1.9 fusion.36
  (45 shorter events, 1.8 us)
Async XLA Ops:
  6.5 69.8 %copy-start = (f32[2]{0:T(128)S(1)}, f32[2]{0:T(128)}, u32[]{:S(2)}) copy-start(f32[2]{0:T(128)} %param.17) | copy-start | bytes 28
  6.5 101.6 %all-gather.5.cloned.1.call-start = ((), (), s32[]{:S(2)}) async-start(), calls=%async_computation.2 | async-start | bytes 1310720 | tf_op jit(solution)/shard_map/all_gather | solution.py:95
  41.7 1.7 copy-start.3
  77.3 1.6 copy-start.6
  78.8 10.9 %copy-start.1 = (bf16[64,2048]{1,0:T(8,128)(2,1)S(1)}, bf16[64,2048]{1,0:T(8,128)(2,1)}, u32[]{:S(2)}) copy-start(bf16[64,2048]{1,0:T(8,128)(2,1)} %param.13) | copy-start | bytes 786436
  78.9 10.9 %copy-start.2 = (f32[2048]{0:T(1024)S(1)}, f32[2048]{0:T(1024)}, u32[]{:S(2)}) copy-start(f32[2048]{0:T(1024)} %param.20) | copy-start | bytes 24580
  78.9 11.2 %copy-start.4 = (f32[2048]{0:T(1024)S(1)}, f32[2048]{0:T(1024)}, u32[]{:S(2)}) copy-start(f32[2048]{0:T(1024)} %param.21) | copy-start | bytes 24580
  91.0 111.6 %all-gather.7.cloned.1.call-start = ((), (), s32[]{:S(2)}) async-start(), calls=%async_computation.3 | async-start | bytes 6488064 | tf_op jit(solution)/shard_map/all_gather | solution.py:98
  91.8 204.3 %all-gather.11.cloned.1.call-start = ((), (), s32[]{:S(2)}) async-start(), calls=%async_computation.5 | async-start | bytes 6488064 | tf_op jit(solution)/shard_map/all_gather | solution.py:106
  92.5 296.1 %all-gather.9.cloned.1.call-start = ((), (), s32[]{:S(2)}) async-start(), calls=%async_computation.4 | async-start | bytes 6488064 | tf_op jit(solution)/shard_map/all_gather | solution.py:99
  93.1 327.5 %reduce-scatter.2.cloned.1.call-start = ((), (), s32[]{:S(2)}) async-start(), calls=%async_computation.6 | async-start | bytes 1310720 | tf_op jit(solution)/shard_map/reduce_scatter | solution.py:109
  108.1 280.5 %copy-start.7 = (bf16[256,2048]{1,0:T(8,128)(2,1)S(1)}, bf16[256,2048]{1,0:T(8,128)(2,1)}, u32[]{:S(2)}) copy-start(bf16[256,2048]{1,0:T(8,128)(2,1)} %all-gather.5.cloned.1.call-done) | copy-start | bytes 3145732
  207.4 214.3 %copy-start.5 = (f32[2048]{0:T(1024)S(1)}, f32[2048]{0:T(1024)}, u32[]{:S(2)}) copy-start(f32[2048]{0:T(1024)} %param.22) | copy-start | bytes 24580
Sparse Core Ops, SparseCore 0:
  91.1 16.9 all-gather.4
  110.3 92.2 all-gather.6
  204.7 91.2 all-gather.10
  298.1 90.4 all-gather.8
  397.6 22.9 reduce-scatter.1
where the time goes:
time: 431 us; the launch traced here: 430 us
  waiting for transfers between devices  316 us (73%)
  blocking collectives  71.5 us (17%)
  matrix products  20.8 us (5%)
  between operations  13.4 us (3%)
  other arithmetic  6.02 us (1%)
    all_gather x1, waiting for transfers between devices, on_device(): lax.all_gather(gate_weight, 'sp', axis=0, tiled=True)  94.5 us
    all_gather x1, waiting for transfers between devices, on_device(): lax.all_gather(up_weight, 'sp', axis=0, tiled=True)  92.6 us
    all_gather x1, waiting for transfers between devices, on_device(): down_whole = lax.all_gather(down_weight, 'sp', axis=1, tiled=True)  88.6 us
    all_gather x1, blocking collectives, on_device(): key_piece = lax.all_gather(key_pairs, 'sp', axis=0, tiled=True)  33 us
    all_gather x1, blocking collectives, on_device(): value_piece = lax.all_gather(values, 'sp', axis=0, tiled=True)  31.3 us
    reduce_scatter x1, waiting for transfers between devices, on_device(): lax.psum_scatter(jnp.dot(picked, down_whole, preferred_element_type=jnp.f...  23.1 us
    all_gather x1, waiting for transfers between devices, on_device(): gathered = lax.all_gather(normed_in, 'tp', axis=0, tiled=True)  15 us
    dot_general x1, matrix products, on_device(): jnp.dot(picked, down_whole, preferred_element_type=jnp.float32)  8.9 us
  transfers between devices with their start and end apart: 5, of which 5 were waited for; matrix products, arithmetic and copies ran while one was open for 1% of the time, Pallas kernels for 0%

commit v1 on v0

--- a/solution.py
+++ b/solution.py
@@ -43,7 +43,9 @@
     )
     state = (empty, empty)
     key_piece = lax.all_gather(key_pairs, "sp", axis=0, tiled=True)
-    value_piece = lax.all_gather(values, "sp", axis=0, tiled=True)
+    value_piece = jnp.concatenate(
+        lax.all_to_all(jnp.stack([values] * lax.axis_size("sp")), "sp", 0, 0), axis=0
+    )
     length = key_piece.shape[0]
     span = length
     for split_count in range(1, length + 1):

time: 431 us -> 412 us (0.956)
  blocking collectives: 71.5 us -> 44.8 us
  starting transfers between devices: 0.16 us -> 7.47 us
    all_gather x1 -> x0, blocking collectives: 31.3 us -> none  [on_device(): value_piece = lax.all_gather(values, 'sp', axis=0, tiled=True)]
    all_to_all x0 -> x1, starting transfers between devices: none -> 7.28 us  [on_device(): lax.all_to_all(jnp.stack([values] * lax.axis_size('sp')), 'sp', 0, 0)]
    all_gather x1, blocking collectives: 33 us -> 37.6 us  [on_device(): key_piece = lax.all_gather(key_pairs, 'sp', axis=0, tiled=True)]
  transfers between devices with their start and end apart: 5 -> 6, of which waited for: 5 -> 5; matrix products, arithmetic and copies ran while one was open for 1% -> 2% of each run, Pallas kernels for 0% -> 0%
where the time goes in v1:
time: 412 us
  waiting for transfers between devices  312 us (76%)
  blocking collectives  44.8 us (11%)
  matrix products  23.1 us (6%)
  between operations  13.4 us (3%)
  starting transfers between devices  7.47 us (2%)
  other arithmetic  5.98 us (1%)
  local copies, waits for them, and re-layouts  5.11 us (1%)
    all_gather x1, waiting for transfers between devices, on_device(): lax.all_gather(gate_weight, 'sp', axis=0, tiled=True)  94.5 us
    all_gather x1, waiting for transfers between devices, on_device(): lax.all_gather(up_weight, 'sp', axis=0, tiled=True)  92.6 us
    all_gather x1, waiting for transfers between devices, on_device(): down_whole = lax.all_gather(down_weight, 'sp', axis=1, tiled=True)  88.6 us
    all_gather x1, blocking collectives, on_device(): key_piece = lax.all_gather(key_pairs, 'sp', axis=0, tiled=True)  37.6 us
    reduce_scatter x1, waiting for transfers between devices, on_device(): lax.psum_scatter(jnp.dot(picked, down_whole, preferred_element_type=jnp.f...  23.2 us
    all_gather x1, waiting for transfers between devices, on_device(): gathered = lax.all_gather(normed_in, 'tp', axis=0, tiled=True)  11.1 us
    dot_general x1, matrix products, on_device(): jnp.dot(picked, down_whole, preferred_element_type=jnp.float32)  8.91 us
  transfers between devices with their start and end apart: 6, of which 5 were waited for; matrix products, arithmetic and copies ran while one was open for 2% of the time, Pallas kernels for 0%

profile of v1, /device:TPU:0, one launch (start us, length us, event | category | flops | bytes accessed | tf_op | source)
XLA Modules:
  0.0 411.7 jit_solution(6058459136460741702)
XLA Ops:
  6.5 1.8 stack.2
  8.3 7.3 %all-to-all-start = ((bf16[8,256,128]{2,1,0:T(8,128)(2,1)}), bf16[8,256,128]{2,1,0:T(8,128)(2,1)S(1)}, u32[]{:S(2)}, u32[]{:S(2)}) async-start(bf16[8,256,128]{2,1,0:T(8,128)(2,1)} %stack.2), calls=%async_computation | async-start | bytes 1048576 | tf_op jit(solution)/shard_map/all_to_all | solution.py:47
  15.6 0.9 copy.16
  16.6 37.6 %all_gather.15 = bf16[2048,128]{0,1:T(8,128)(2,1)S(1)} all-gather(bf16[256,128]{0,1:T(8,128)(2,1)S(1)} %copy.16), channel_id=1, replica_groups=mesh['sp'=8,'tp'=4] {'sp'}, dimensions={0}, use_global_device_ids=true | all-gather | bytes 589824 | tf_op jit(solution)/shard_map/all_gather | solution.py:45
  54.2 1.0 copy.14
  55.3 0.8 multiply_reduce_fusion.1
  56.3 0.8 multiply_reduce_fusion
  57.2 0.8 fusion
  58.1 0.8 fusion.2
  59.4 3.2 fusion.29
  62.9 1.4 multiply_reduce_fusion.4
  64.7 7.2 %all_to_all.20 = bf16[4,64,256]{2,1,0:T(8,128)(2,1)S(1)} all-to-all(bf16[4,64,256]{2,1,0:T(8,128)(2,1)S(1)} %reshape_reshape.4), channel_id=1, replica_groups=mesh['sp'=8,'tp'=4] {'tp'}, dimensions={0} | all-to-all | bytes 262144 | tf_op jit(solution)/shard_map/all_to_all | solution.py:91
  72.1 3.2 multiply_reduce_fusion.3
  75.5 0.9 multiply_convert_fusion
  76.5 0.7 all-gather.7.cloned.1.call-update
  78.6 11.1 %all-gather.5.cloned.1.call-done = bf16[256,2048]{1,0:T(8,128)(2,1)} async-done(((bf16[64,2048]{1,0:T(8,128)(2,1)}), bf16[256,2048]{1,0:T(8,128)(2,1)}) %all-gather.5.cloned.1.call-update) | async-done | bytes 1048592 | tf_op jit(solution)/shard_map/all_gather | solution.py:97
  89.6 94.5 %all-gather.7.cloned.1.call-done = bf16[2048,1408]{1,0:T(8,128)(2,1)} async-done(((bf16[256,1408]{1,0:T(8,128)(2,1)}), bf16[2048,1408]{1,0:T(8,128)(2,1)}) %all-gather.7.cloned.1.call-update) | async-done | bytes 5767184 | tf_op jit(solution)/shard_map/all_gather | solution.py:100
  184.1 4.8 %fusion.45 = f32[256,1408]{1,0:T(8,128)S(1)} fusion(bf16[256,2048]{1,0:T(8,128)(2,1)} %all-gather.5.cloned.1.call-done, bf16[2048,1408]{1,0:T(8,128)(2,1)} %all-gather.7.cloned.1.call-done), kind=kOutput, calls=%fused_computation.58 | convolution fusion | flops 1476395008 | bytes 8257536 | tf_op jit(solution)/shard_map/dot_general | solution.py:104
  188.9 88.6 %all-gather.11.cloned.1.call-done = bf16[1408,2048]{1,0:T(8,128)(2,1)} async-done(((bf16[1408,256]{1,0:T(8,128)(2,1)}), bf16[1408,2048]{1,0:T(8,128)(2,1)}) %all-gather.11.cloned.1.call-update) | async-done | bytes 5767184 | tf_op jit(solution)/shard_map/all_gather | solution.py:108
  277.5 92.6 %all-gather.9.cloned.1.call-done = bf16[2048,1408]{1,0:T(8,128)(2,1)} async-done(((bf16[256,1408]{1,0:T(8,128)(2,1)}), bf16[2048,1408]{1,0:T(8,128)(2,1)}) %all-gather.9.cloned.1.call-update) | async-done | bytes 5767184 | tf_op jit(solution)/shard_map/all_gather | solution.py:101
  370.1 8.9 %convolution_convert_fusion = bf16[256,2048]{1,0:T(8,128)(2,1)} fusion(bf16[1408,2048]{1,0:T(8,128)(2,1)} %all-gather.11.cloned.1.call-done, bf16[256,2048]{1,0:T(8,128)(2,1)S(1)} %copy-done.9, bf16[2048,1408]{1,0:T(8,128)(2,1)} %all-gather.9.cloned.1.call-done, f32[256,1408]{1,0:T(8,128)S(1)} %fusion.45), kind=kOutput, calls=%fused_computation.10 | convolution fusion | flops 2955476992 | bytes 15073280 | tf_op jit(solution)/shard_map/dot_general | solution.py:112
  379.0 23.2 %reduce-scatter.2.cloned.1.call-done = bf16[64,2048]{1,0:T(8,128)(2,1)} async-done(((bf16[256,2048]{1,0:T(8,128)(2,1)}), bf16[64,2048]{1,0:T(8,128)(2,1)}) %reduce-scatter.2.cloned.1.call-update) | async-done | bytes 262160 | tf_op jit(solution)/shard_map/reduce_scatter | solution.py:111
  402.2 1.1 fusion.32
  403.3 1.9 fusion.36
  (51 shorter events, 3.3 us)
Async XLA Ops:
  6.5 50.5 %copy-start = (f32[2]{0:T(128)S(1)}, f32[2]{0:T(128)}, u32[]{:S(2)}) copy-start(f32[2]{0:T(128)} %param.17) | copy-start | bytes 28
  8.3 51.1 %all-to-all-start = ((bf16[8,256,128]{2,1,0:T(8,128)(2,1)}), bf16[8,256,128]{2,1,0:T(8,128)(2,1)S(1)}, u32[]{:S(2)}, u32[]{:S(2)}) async-start(bf16[8,256,128]{2,1,0:T(8,128)(2,1)} %stack.2), calls=%async_computation | async-start | bytes 1048576 | tf_op jit(solution)/shard_map/all_to_all | solution.py:47
  15.6 74.1 %all-gather.5.cloned.1.call-start = ((), (), s32[]{:S(2)}) async-start(), calls=%async_computation.3 | async-start | bytes 1310720 | tf_op jit(solution)/shard_map/all_gather | solution.py:97
  56.1 1.9 copy-start.1
  57.1 2.3 copy-start.2
  59.4 3.5 copy-start.3
  62.6 1.7 copy-start.8
  64.3 10.9 %copy-start.4 = (bf16[64,2048]{1,0:T(8,128)(2,1)S(1)}, bf16[64,2048]{1,0:T(8,128)(2,1)}, u32[]{:S(2)}) copy-start(bf16[64,2048]{1,0:T(8,128)(2,1)} %param.13) | copy-start | bytes 786436
  64.3 10.9 %copy-start.5 = (f32[2048]{0:T(1024)S(1)}, f32[2048]{0:T(1024)}, u32[]{:S(2)}) copy-start(f32[2048]{0:T(1024)} %param.20) | copy-start | bytes 24580
  64.3 11.2 %copy-start.6 = (f32[2048]{0:T(1024)S(1)}, f32[2048]{0:T(1024)}, u32[]{:S(2)}) copy-start(f32[2048]{0:T(1024)} %param.21) | copy-start | bytes 24580
  76.5 107.7 %all-gather.7.cloned.1.call-start = ((), (), s32[]{:S(2)}) async-start(), calls=%async_computation.4 | async-start | bytes 6488064 | tf_op jit(solution)/shard_map/all_gather | solution.py:100
  77.2 200.3 %all-gather.11.cloned.1.call-start = ((), (), s32[]{:S(2)}) async-start(), calls=%async_computation.6 | async-start | bytes 6488064 | tf_op jit(solution)/shard_map/all_gather | solution.py:108
  77.9 292.2 %all-gather.9.cloned.1.call-start = ((), (), s32[]{:S(2)}) async-start(), calls=%async_computation.5 | async-start | bytes 6488064 | tf_op jit(solution)/shard_map/all_gather | solution.py:101
  78.5 323.7 %reduce-scatter.2.cloned.1.call-start = ((), (), s32[]{:S(2)}) async-start(), calls=%async_computation.7 | async-start | bytes 1310720 | tf_op jit(solution)/shard_map/reduce_scatter | solution.py:111
  89.6 280.5 %copy-start.9 = (bf16[256,2048]{1,0:T(8,128)(2,1)S(1)}, bf16[256,2048]{1,0:T(8,128)(2,1)}, u32[]{:S(2)}) copy-start(bf16[256,2048]{1,0:T(8,128)(2,1)} %all-gather.5.cloned.1.call-done) | copy-start | bytes 3145732
  188.9 214.4 %copy-start.7 = (f32[2048]{0:T(1024)S(1)}, f32[2048]{0:T(1024)}, u32[]{:S(2)}) copy-start(f32[2048]{0:T(1024)} %param.22) | copy-start | bytes 24580
Sparse Core Ops, SparseCore 0:
  76.6 13.0 all-gather.4
  91.8 92.2 all-gather.6
  186.2 91.2 all-gather.10
  279.6 90.4 all-gather.8
  379.2 22.9 reduce-scatter.1
